TPU v7x, 256 devices: a 4x2x16 block of a 4x16x16 slice. The times are simulated.
256 devices in a mesh: grp: 2 (over y), sp: 16 (over z), tp: 8 (over x, core).
Axes of the slice: x: 4, y: 2, z: 16, core: 2. Of those that a mesh axis runs over, the one named last changes fastest.
The devices are a block of a 4x16x16 slice.
Arguments:
- latent: bfloat16 [49152, 2048], P(('grp', 'sp')), parts along dimension 0, may hold values from -6 to 6
- condition: bfloat16 [4096], P('grp'), parts along dimension 0, may hold values from -6 to 6
- context_tokens: bfloat16 [512, 2048], P(('grp', 'sp')), parts along dimension 0, may hold values from -6 to 6
- context_condition: bfloat16 [2048], replicated, may hold values from -6 to 6
- shift_weight: bfloat16 [2048, 2048], P('sp', 'tp'), may hold values from -0.25 to 0.25
- scale_weight: bfloat16 [2048, 2048], P('sp', 'tp'), may hold values from -0.25 to 0.25
- gate_weight: bfloat16 [2048, 2048], P('sp', 'tp'), may hold values from -0.25 to 0.25
- norm_gain: bfloat16 [2048], replicated, may hold values from 0.099609375 to 1.8984375
- query_weight: bfloat16 [2048, 1024], P(None, 'tp'), may hold values from -0.125 to 0.125
- key_weight: bfloat16 [2048, 1024], P(None, 'tp'), may hold values from -0.125 to 0.125
- value_weight: bfloat16 [2048, 1024], P(None, 'tp'), may hold values from -0.125 to 0.125
- out_weight: bfloat16 [1024, 2048], replicated, may hold values from -0.1875 to 0.1875
- offset_bias: float32 [16, 15, 31], P('tp'), may hold values from 0.5 to 260
Outputs:
- mixed_latent: bfloat16 [49152, 2048], P(('grp', 'sp', 'tp')), parts along dimension 0
There are 2 independent parts, one for each index of `grp`. A program takes and returns all parts, laid end to end along the dimension named above; an argument that names none is the same for every part. Nothing has to cross between parts.
All inputs are finite; a program needn't handle non-finite values.
Results may differ from a plain program's by a relative error of at most 0.011.
Values may be sent and summed in bfloat16 or wider, within the bound.
A program may use at most 128 MiB of HBM per device.

v0:
```python
import functools

import jax
import jax.numpy as jnp
from jax import lax
from jax.experimental import pallas as pl
from jax.experimental.pallas import tpu as pltpu
from jax.sharding import PartitionSpec as P

HEAD_DIM = 64
GRID_W = 64
WIN_ROWS = 8
WIN_COLS = 16
COL_BLOCK = 16
STRIP = COL_BLOCK + WIN_COLS
BLOCKS = GRID_W // COL_BLOCK
HALO = WIN_ROWS // 2
STARTS = (0, 8, 24, 32)
VARIANT = (0, 1, 1, 2)
SHIFTS = (15, 7, -1)
EPS = 1e-6
MASKED = -1e30
LANES = 128

bf16 = jnp.bfloat16
f32 = jnp.float32
MESH = pl.DeviceIdType.MESH


def dot(a, b):
    return jnp.dot(a, b, preferred_element_type=f32)


def dot_nt(a, b):
    return lax.dot_general(a, b, (((1,), (1,)), ((), ())), preferred_element_type=f32)


def kernel(
    n_sp,
    n_tp,
    latent,
    cond,
    ctx_tokens,
    ctx_cond,
    shift_w,
    scale_w,
    gate_w,
    gain,
    query_w,
    key_w,
    value_w,
    out_w,
    bias,
    out,
    X,
    CD,
    XD,
    CT,
    MW,
    GN,
    W,
    W2,
    WO,
    BI,
    PAD,
    TP,
    TB,
    RS,
    P1,
    R1,
    P2,
    R2,
    LH,
    CS,
    CR,
    CV,
    QS,
    KS,
    VS,
    HB,
    HR,
    AS,
    AR,
    OB,
    load_sem,
    p1_send,
    p1_recv,
    p2_send,
    p2_recv,
    c_send,
    c_recv,
    h_send,
    h_recv,
    a_send,
    a_recv,
    o_sem,
):
    sp = lax.axis_index("sp")
    tp = lax.axis_index("tp")
    tokens, width = X.shape
    ft = width // n_tp
    rows = tokens // GRID_W
    crows = rows // n_tp
    share = crows * GRID_W
    urows = crows + WIN_ROWS - 1
    ukeys = urows * STRIP
    qrows = crows * 2 * COL_BLOCK
    att = W.shape[1] // 3

    barrier = pltpu.get_barrier_semaphore()

    def greet_sp(k, c):
        pl.semaphore_signal(
            barrier, inc=1, device_id={"sp": lax.rem(sp + k, n_sp)}, device_id_type=MESH
        )
        return c

    def greet_tp(k, c):
        pl.semaphore_signal(
            barrier, inc=1, device_id={"tp": lax.rem(tp + k, n_tp)}, device_id_type=MESH
        )
        return c

    lax.fori_loop(1, n_sp, greet_sp, 0)
    lax.fori_loop(1, n_tp, greet_tp, 0)

    loads = [
        (cond, CD),
        (ctx_cond, XD),
        (shift_w, MW.at[0]),
        (scale_w, MW.at[1]),
        (gate_w, MW.at[2]),
        (bias, BI),
        (gain, GN),
        (ctx_tokens, CT),
        (latent, X),
        (query_w, W.at[:, pl.ds(0, att)]),
        (key_w, W.at[:, pl.ds(att, att)]),
        (value_w, W.at[:, pl.ds(2 * att, att)]),
        (out_w, WO),
    ]
    loads = [
        pltpu.make_async_copy(src, dst, load_sem.at[i]) for i, (src, dst) in enumerate(loads)
    ]
    for copy in loads:
        copy.start()

    row8 = lax.broadcasted_iota(jnp.int32, (8, ft), 0)

    for copy in loads[:5]:
        copy.wait()

    def own_act(ref):
        v = ref[...].astype(f32)
        act = (v / (1.0 + jnp.exp(-v))).astype(bf16).astype(f32)
        own = lax.broadcasted_iota(jnp.int32, act.shape, 0) == sp
        return jnp.sum(jnp.where(own, act, 0.0), axis=0, keepdims=True)

    own_cond, own_ctx = own_act(CD), own_act(XD)
    r16 = lax.broadcasted_iota(jnp.int32, (16, own_cond.shape[1]), 0)
    acts = jnp.where(r16 == 0, own_cond, jnp.where(r16 == 1, own_ctx, 0.0)).astype(bf16)
    d_shift, d_scale, d_gate = dot(acts, MW[0]), dot(acts, MW[1]), dot(acts, MW[2])
    terms = (d_shift[0:1], d_scale[0:1], d_gate[0:1], d_shift[1:2], d_scale[1:2])
    packed = jnp.zeros((8, ft), f32)
    for i, term in enumerate(terms):
        packed = jnp.where(row8 == i, term, packed)
    P1[...] = packed
    R1[sp] = packed

    pl.semaphore_wait(barrier, n_sp - 1 + n_tp - 1)

    def p1_copy(k):
        peer = lax.rem(sp + k, n_sp)
        return pltpu.make_async_remote_copy(
            src_ref=P1,
            dst_ref=R1.at[sp],
            send_sem=p1_send.at[peer],
            recv_sem=p1_recv.at[sp],
            device_id={"sp": peer},
            device_id_type=MESH,
        )

    def p1_arrival(k):
        peer = lax.rem(sp + k, n_sp)
        return pltpu.make_async_remote_copy(
            src_ref=P1,
            dst_ref=R1.at[peer],
            send_sem=p1_send.at[peer],
            recv_sem=p1_recv.at[peer],
            device_id={"sp": peer},
            device_id_type=MESH,
        )

    def p1_start(k, c):
        p1_copy(k).start()
        return c

    lax.fori_loop(1, n_sp, p1_start, 0)

    loads[5].wait()
    lane = lax.broadcasted_iota(jnp.int32, (COL_BLOCK, LANES), 1)
    in_group = lax.rem(lane, STRIP)
    query = lax.broadcasted_iota(jnp.int32, (COL_BLOCK, LANES), 0)
    lower = (
        jnp.maximum(query - WIN_COLS // 2, 0),
        query,
        jnp.minimum(query + WIN_COLS // 2, WIN_COLS),
    )
    inside = [(in_group >= lo) & (in_group < lo + WIN_COLS) for lo in lower]
    offsets = 2 * WIN_ROWS - 1
    PAD[...] = jnp.zeros_like(PAD)
    for h in range(2):
        PAD[h, pl.ds(0, offsets), pl.ds(0, 2 * WIN_COLS - 1)] = BI[h]
        x = PAD[h]
        x = x + pltpu.roll(x, 32, 1)
        PAD[h] = x + pltpu.roll(x, 64, 1)

    def lay_out(o, c):
        for h in range(2):
            line = jnp.broadcast_to(PAD[h, pl.ds(o, 1), :], (COL_BLOCK, LANES))
            for v in range(3):
                turned = pltpu.roll(line, (-SHIFTS[v]) % LANES, 1, stride=1, stride_axis=0)
                TP[v, h, o] = jnp.where(inside[v], turned, MASKED)
        return c

    lax.fori_loop(0, offsets, lay_out, 0)
    group = lane // STRIP
    per = LANES // STRIP
    variants = (
        (-HALO, lambda i: i),
        (0, lambda i: 0),
        (-crows, lambda i: max(crows + i - HALO, 0)),
        (-(urows - crows), lambda i: urows - WIN_ROWS),
    )

    def assemble(vh, c):
        v, h = vh // 2, lax.rem(vh, 2)
        for rv, (delta, first) in enumerate(variants):
            for i in range(crows):
                for g in range(TB.shape[-1] // LANES):
                    tile = jnp.full((COL_BLOCK, LANES), MASKED, f32)
                    for l in range(per):
                        j = g * per + l
                        if first(i) <= j < first(i) + WIN_ROWS and j < urows:
                            o = delta + j - i + WIN_ROWS - 1
                            tile = jnp.where(group == l, TP[v, h, o], tile)
                    TB[rv, v, i, h, :, pl.ds(g * LANES, LANES)] = tile
        return c

    lax.fori_loop(0, 6, assemble, 0)

    loads[8].wait()

    def norms(k, c):
        at = pl.ds(pl.multiple_of(k * 16, 16), 16)
        x = X[at, :].astype(f32)
        mean = jnp.sum(x * x, axis=1, keepdims=True) * (1.0 / width)
        RS[at, :] = jnp.broadcast_to(lax.rsqrt(mean + EPS), (16, LANES))
        return c

    lax.fori_loop(0, tokens // 16, norms, 0)
    loads[6].wait()
    loads[7].wait()
    for copy in loads[9:12]:
        copy.wait()

    CV[:, pl.ds(LANES, LANES)] = jnp.ones((CV.shape[0], LANES), bf16)

    def fill(r, c):
        for b in range(BLOCKS):
            VS[b, r, :, pl.ds(LANES, LANES)] = jnp.ones((STRIP, LANES), bf16)
        return c

    lax.fori_loop(0, rows + 2 * HALO, fill, 0)

    def p1_wait(k, c):
        p1_arrival(k).wait_recv()
        return c

    lax.fori_loop(1, n_sp, p1_wait, 0)
    summed = jnp.sum(R1[...], axis=0)
    P2[...] = summed
    R2[tp] = summed

    def p2_copy(k, slot):
        peer = lax.rem(tp + k, n_tp)
        return pltpu.make_async_remote_copy(
            src_ref=P2,
            dst_ref=R2.at[tp if slot is None else peer],
            send_sem=p2_send.at[peer],
            recv_sem=p2_recv.at[tp if slot is None else peer],
            device_id={"tp": peer},
            device_id_type=MESH,
        )

    def p2_start(k, c):
        p2_copy(k, None).start()
        return c

    lax.fori_loop(1, n_tp, p2_start, 0)

    def p2_wait(k, c):
        p2_copy(k, 1).wait_recv()
        return c

    lax.fori_loop(1, n_tp, p2_wait, 0)

    ctx_rows = CT.shape[0]
    sq = jnp.zeros((ctx_rows, 1), f32)
    for t in range(n_tp):
        x = CT[:, pl.ds(t * ft, ft)].astype(f32)
        sq = sq + jnp.sum(x * x, axis=1, keepdims=True)
    ctx_scale = lax.rsqrt(sq * (1.0 / width) + EPS)
    r16 = lax.broadcasted_iota(jnp.int32, (16, ft), 0)
    for t in range(n_tp):
        cols = pl.ds(t * ft, ft)
        x = CT[:, cols].astype(f32) * ctx_scale
        x = x * GN[pl.ds(t, 1), :].astype(f32) * (1.0 + R2[t, 4:5, :]) + R2[t, 3:4, :]
        LH[pl.ds(0, ctx_rows), cols] = x.astype(bf16)
        shift = R2[t, 0:1, :]
        high = shift.astype(bf16).astype(f32)
        low = shift - high
        pair = jnp.where(r16 == 0, high, jnp.where(r16 == 1, low, 0.0))
        LH[pl.ds(ctx_rows, 16), cols] = pair.astype(bf16)
    side = dot(LH[...], W[...])
    CS[...] = side[:ctx_rows, att:].astype(bf16)
    add = side[ctx_rows : ctx_rows + 1] + side[ctx_rows + 1 : ctx_rows + 2]

    def c_copy(k, slot):
        peer = lax.rem(sp + k, n_sp)
        return pltpu.make_async_remote_copy(
            src_ref=CS,
            dst_ref=CR.at[sp if slot is None else peer],
            send_sem=c_send.at[peer],
            recv_sem=c_recv.at[sp if slot is None else peer],
            device_id={"sp": peer},
            device_id_type=MESH,
        )

    def c_start(k, c):
        c_copy(k, None).start()
        return c

    lax.fori_loop(1, n_sp, c_start, 0)
    CR[sp] = CS[...]

    halves = ft // LANES
    scale = jnp.concatenate([R2[t, 1:2, :] for t in range(n_tp)], axis=0)
    factor = GN[...].astype(f32) * (1.0 + scale)
    slabs = [factor[:, s * LANES : (s + 1) * LANES] for s in range(halves)]
    slabs.append(jnp.zeros((LANES - halves * n_tp, LANES), f32))
    turned = jnp.concatenate(slabs, axis=0).T
    for s in range(halves):
        for t in range(n_tp):
            at = pl.ds(t * ft + s * LANES, LANES)
            column = turned[:, s * n_tp + t : s * n_tp + t + 1]
            W2[at, :] = (W[at, :].astype(f32) * column).astype(bf16)

    per_block = HALO * GRID_W
    steps = rows // HALO
    head0 = lax.broadcasted_iota(jnp.int32, (COL_BLOCK, LANES), 1) < HEAD_DIM

    def h_copy(side_):
        return pltpu.make_async_remote_copy(
            src_ref=HB.at[side_],
            dst_ref=HR.at[side_],
            send_sem=h_send.at[side_],
            recv_sem=h_recv.at[side_],
            device_id={"sp": lax.rem(sp + (1 if side_ == 0 else n_sp - 1), n_sp)},
            device_id_type=MESH,
        )

    def project(k, c):
        m = jnp.where(k == 0, 0, jnp.where(k == 1, steps - 1, k - 1))
        at = pl.ds(pl.multiple_of(m * per_block, per_block), per_block)
        acc = dot(X[at, :], W2[...])
        rs = RS[at, :]
        parts = [
            acc[:, p * att : (p + 1) * att] * rs + add[:, p * att : (p + 1) * att]
            for p in range(3)
        ]
        q = parts[0] * (HEAD_DIM**-0.5)
        for r in range(HALO):
            for b in range(BLOCKS):
                begin = r * GRID_W + b * COL_BLOCK
                piece = q[begin : begin + COL_BLOCK]
                QS[b, m * HALO + r, 0] = jnp.where(head0, piece, 0.0).astype(bf16)
                QS[b, m * HALO + r, 1] = jnp.where(head0, 0.0, piece).astype(bf16)
                begin = r * GRID_W + STARTS[b]
                KS[b, m * HALO + r + HALO] = parts[1][begin : begin + STRIP].astype(bf16)
                VS[b, m * HALO + r + HALO, :, pl.ds(0, LANES)] = parts[2][
                    begin : begin + STRIP
                ].astype(bf16)

        @pl.when(k < 2)
        def _():
            HB[1 - k, :, pl.ds(0, att)] = parts[1].astype(bf16)
            HB[1 - k, :, pl.ds(att, att)] = parts[2].astype(bf16)

        return c

    lax.fori_loop(0, 2, project, 0)

    @pl.when(sp < n_sp - 1)
    def _():
        h_copy(0).start()

    @pl.when(sp > 0)
    def _():
        h_copy(1).start()

    lax.fori_loop(2, steps, project, 0)

    def c_wait(k, c):
        c_copy(k, 1).wait_recv()
        return c

    lax.fori_loop(1, n_sp, c_wait, 0)
    for s in range(n_sp):
        CV[pl.ds(s * ctx_rows, ctx_rows), pl.ds(0, att)] = CR[s, :, pl.ds(att, att)]

    loads[12].wait()

    def spread(side_):
        first = 0 if side_ == 0 else rows + HALO
        for r in range(HALO):
            pair = HR[side_, pl.ds(r * GRID_W, GRID_W), :].astype(f32)
            for b in range(BLOCKS):
                strip = pair[STARTS[b] : STARTS[b] + STRIP].astype(bf16)
                KS[b, first + r] = strip[:, :att]
                VS[b, first + r, :, pl.ds(0, LANES)] = strip[:, att:]

    def a_copy(c, slot):
        return pltpu.make_async_remote_copy(
            src_ref=AS.at[c],
            dst_ref=AR.at[tp if slot is None else c],
            send_sem=a_send.at[c],
            recv_sem=a_recv.at[tp if slot is None else c],
            device_id={"tp": c},
            device_id_type=MESH,
        )

    low = -(-HALO // crows)
    inner = n_tp - 2 * low
    outer = 2 * low

    def attend(k, carry):
        @pl.when(k == inner)
        def _():
            @pl.when(sp > 0)
            def _():
                h_copy(0).wait_recv()
                spread(0)

            @pl.when(sp < n_sp - 1)
            def _():
                h_copy(1).wait_recv()
                spread(1)

        e = lax.rem(tp + 1 + k, outer)
        c = jnp.where(
            k < inner, low + lax.rem(tp + k, inner), jnp.where(e < low, e, e + inner)
        )
        rv = jnp.where(
            (sp == 0) & (c < 2), c + 1, jnp.where((sp == n_sp - 1) & (c == n_tp - 1), 3, 0)
        )
        base = jnp.where(
            (rv == 1) | (rv == 2), HALO, jnp.where(rv == 3, rows + HALO - urows, c * crows)
        )
        for b in range(BLOCKS):
            q2 = QS[b, pl.ds(c * crows, crows)].reshape(qrows, LANES)
            ks = KS[b, pl.ds(base, urows)].reshape(ukeys, LANES)
            near = dot_nt(q2, ks)
            table = TB[rv, VARIANT[b], :, :, :, pl.ds(0, ukeys)].reshape(qrows, ukeys)
            near = near + table
            far = dot_nt(q2, CR[:, :, pl.ds(0, att)].reshape(n_sp * ctx_rows, att))
            peak = jnp.maximum(
                jnp.max(near, axis=1, keepdims=True), jnp.max(far, axis=1, keepdims=True)
            )
            near = jnp.exp(near - peak).astype(bf16)
            far = jnp.exp(far - peak).astype(bf16)
            vs = VS[b, pl.ds(base, urows)].reshape(ukeys, 2 * LANES)
            both = dot(near, vs) + dot(far, CV[...])
            value = (both[:, :LANES] / both[:, LANES:]).reshape(crows, 2, COL_BLOCK, LANES)
            for i in range(crows):
                AS[c, pl.ds(i * GRID_W + b * COL_BLOCK, COL_BLOCK), :] = jnp.where(
                    head0, value[i, 0], value[i, 1]
                ).astype(bf16)

        @pl.when(c != tp)
        def _():
            a_copy(c, None).start()

        return carry

    lax.fori_loop(0, n_tp, attend, 0)

    AR[tp] = AS[tp]

    def a_wait(k, c):
        a_copy(lax.rem(tp + k, n_tp), 1).wait_recv()
        return c

    lax.fori_loop(1, n_tp, a_wait, 0)
    merged = jnp.concatenate([AR[t] for t in range(n_tp)], axis=1)
    own = pl.ds(pl.multiple_of(tp * share, share), share)
    stores = []
    for t in range(n_tp):
        cols = pl.ds(t * ft, ft)
        branch = dot(merged, WO[:, cols])
        OB[:, cols] = (X[own, cols].astype(f32) + R2[t, 2:3, :] * branch).astype(bf16)
        store = pltpu.make_async_copy(OB.at[:, cols], out.at[:, cols], o_sem.at[t])
        store.start()
        stores.append(store)

    def p1_done(k, c):
        p1_copy(k).wait_send()
        c_copy(k, None).wait_send()
        return c

    lax.fori_loop(1, n_sp, p1_done, 0)

    def p2_done(k, c):
        p2_copy(k, None).wait_send()
        a_copy(lax.rem(tp + k, n_tp), None).wait_send()
        return c

    lax.fori_loop(1, n_tp, p2_done, 0)

    @pl.when(sp < n_sp - 1)
    def _():
        h_copy(0).wait_send()

    @pl.when(sp > 0)
    def _():
        h_copy(1).wait_send()

    for store in stores:
        store.wait()


def local(n_sp, n_tp, *args):
    (
        latent,
        condition,
        context_tokens,
        context_condition,
        shift_weight,
        scale_weight,
        gate_weight,
        norm_gain,
        query_weight,
        key_weight,
        value_weight,
        out_weight,
        offset_bias,
    ) = args
    tokens, width = latent.shape
    inputs, ft = shift_weight.shape
    att = query_weight.shape[1]
    rows = tokens // GRID_W
    crows = rows // n_tp
    share = crows * GRID_W
    urows = crows + WIN_ROWS - 1
    ctx_rows = context_tokens.shape[0]
    table = -(-urows * STRIP // LANES) * LANES
    padded = rows + 2 * HALO
    operands = (
        latent,
        condition.reshape(n_sp, inputs),
        context_tokens,
        context_condition.reshape(n_sp, inputs),
        shift_weight,
        scale_weight,
        gate_weight,
        norm_gain.reshape(n_tp, ft),
        query_weight,
        key_weight,
        value_weight,
        out_weight,
        offset_bias,
    )
    dma = pltpu.SemaphoreType.DMA
    scratch = [
        pltpu.VMEM((tokens, width), bf16),
        pltpu.VMEM((n_sp, inputs), bf16),
        pltpu.VMEM((n_sp, inputs), bf16),
        pltpu.VMEM((ctx_rows, width), bf16),
        pltpu.VMEM((3, inputs, ft), bf16),
        pltpu.VMEM((n_tp, ft), bf16),
        pltpu.VMEM((width, 3 * att), bf16),
        pltpu.VMEM((width, 3 * att), bf16),
        pltpu.VMEM(out_weight.shape, bf16),
        pltpu.VMEM(offset_bias.shape, f32),
        pltpu.VMEM((2, 16, LANES), f32),
        pltpu.VMEM((3, 2, 2 * WIN_ROWS, COL_BLOCK, LANES), f32),
        pltpu.VMEM((4, 3, crows, 2, COL_BLOCK, table), f32),
        pltpu.VMEM((tokens, LANES), f32),
        pltpu.VMEM((8, ft), f32),
        pltpu.VMEM((n_sp, 8, ft), f32),
        pltpu.VMEM((8, ft), f32),
        pltpu.VMEM((n_tp, 8, ft), f32),
        pltpu.VMEM((ctx_rows + 16, width), bf16),
        pltpu.VMEM((ctx_rows, 2 * att), bf16),
        pltpu.VMEM((n_sp, ctx_rows, 2 * att), bf16),
        pltpu.VMEM((n_sp * ctx_rows, 2 * LANES), bf16),
        pltpu.VMEM((BLOCKS, rows, 2, COL_BLOCK, LANES), bf16),
        pltpu.VMEM((BLOCKS, padded, STRIP, LANES), bf16),
        pltpu.VMEM((BLOCKS, padded, STRIP, 2 * LANES), bf16),
        pltpu.VMEM((2, HALO * GRID_W, 2 * att), bf16),
        pltpu.VMEM((2, HALO * GRID_W, 2 * att), bf16),
        pltpu.VMEM((n_tp, share, LANES), bf16),
        pltpu.VMEM((n_tp, share, LANES), bf16),
        pltpu.VMEM((share, width), bf16),
        dma((13,)),
        dma((n_sp,)),
        dma((n_sp,)),
        dma((n_tp,)),
        dma((n_tp,)),
        dma((n_sp,)),
        dma((n_sp,)),
        dma((2,)),
        dma((2,)),
        dma((n_tp,)),
        dma((n_tp,)),
        dma((n_tp,)),
    ]
    return pl.pallas_call(
        functools.partial(kernel, n_sp, n_tp),
        out_shape=jax.ShapeDtypeStruct((share, width), bf16),
        in_specs=[pl.BlockSpec(memory_space=pl.ANY)] * len(operands),
        out_specs=pl.BlockSpec(memory_space=pl.ANY),
        scratch_shapes=scratch,
        compiler_params=pltpu.CompilerParams(
            collective_id=0, has_side_effects=True, vmem_limit_bytes=60 * 1024 * 1024
        ),
    )(*operands)


def solution(mesh):
    placed = (
        P(("grp", "sp"), None),
        P("grp"),
        P(("grp", "sp"), None),
        P(),
        P("sp", "tp"),
        P("sp", "tp"),
        P("sp", "tp"),
        P(),
        P(None, "tp"),
        P(None, "tp"),
        P(None, "tp"),
        P(),
        P("tp", None, None),
    )
    return jax.shard_map(
        functools.partial(local, mesh.shape["sp"], mesh.shape["tp"]),
        mesh=mesh,
        in_specs=placed,
        out_specs=P(("grp", "sp", "tp"), None),
        check_vma=False,
    )
```

profile of v0, /device:TPU:33, one launch (start us, length us, event | category | flops | bytes accessed | tf_op | source)
XLA Modules:
  0.0 69.9 jit_solution(5032843715906264847)
XLA Ops:
  0.0 1.3 %reshape.11.gain = bf16[8,256]{1,0:T(8,128)(2,1)} reshape(bf16[2048]{0:T(1024)(128)(2,1)} %param.20) | data formatting | bytes 8192 | tf_op jit(solution)/shard_map/reshape | solution.py:576
  1.3 1.3 %copy.14.bias = f32[2,15,31]{2,1,0:T(8,128)} copy(f32[2,15,31]{2,0,1:T(2,128)} %param.25) | data formatting | bytes 7440 | tf_op args[12]
  2.6 65.2 %shard_map.127 = bf16[192,2048]{1,0:T(8,128)(2,1)} custom-call(bf16[1536,2048]{1,0:T(8,128)(2,1)} %latent.1, bf16[16,128]{1,0:T(8,128)(2,1)} %bitcast.2, bf16[16,2048]{1,0:T(8,128)(2,1)} %ctx_tokens.1, bf16[16,128]{1,0:T(8,128)(2,1)} %bitcast.3, bf16[128,256]{1,0:T(8,128)(2,1)} %shift_w.1, bf16[128,256]{1,0:T(8,128)(2,1)} %scale_w.1, ...), custom_call_target="tpu_custom_call" | custom-call | tf_op jit(solution)/shard_map/pallas_call | solution.py:628
  67.8 2.1 %copy.16 = bf16[192,2048]{1,0:T(8,128)(2,1)} copy(bf16[192,2048]{1,0:T(8,128)(2,1)} %shard_map.127) | data formatting | bytes 1572864
where the time goes:
time: 70.4 us; the launch traced here: 69.9 us
  Pallas kernels  65.2 us (93%)
  local copies, waits for them, and re-layouts  4.69 us (7%)
    pallas_call x1, Pallas kernels, local(): pl.pallas_call(functools.partial(kernel, n_sp, n_tp), out_shape=jax.Shape...  65.2 us
    unnamed x2, local copies, waits for them, and re-layouts  3.41 us

commit v1 on v0

--- a/solution.py
+++ b/solution.py
@@ -55,7 +55,6 @@
     X,
     CD,
     XD,
-    CT,
     MW,
     GN,
     W,
@@ -71,8 +70,9 @@
     P2,
     R2,
     LH,
-    CS,
-    CR,
+    W3,
+    CX,
+    CK,
     CV,
     QS,
     KS,
@@ -89,6 +89,13 @@
     p2_recv,
     c_send,
     c_recv,
+    x_send,
+    x_recv,
+    d_send,
+    d_recv,
+    t_send,
+    t_recv,
+    ready,
     h_send,
     h_recv,
     a_send,
@@ -109,10 +116,8 @@
 
     barrier = pltpu.get_barrier_semaphore()
 
-    def greet_sp(k, c):
-        pl.semaphore_signal(
-            barrier, inc=1, device_id={"sp": lax.rem(sp + k, n_sp)}, device_id_type=MESH
-        )
+    def greet_sp(j, c):
+        pl.semaphore_signal(barrier, inc=1, device_id={"sp": j}, device_id_type=MESH)
         return c
 
     def greet_tp(k, c):
@@ -121,18 +126,19 @@
         )
         return c
 
-    lax.fori_loop(1, n_sp, greet_sp, 0)
+    lax.fori_loop(sp + 1, n_sp, greet_sp, 0)
     lax.fori_loop(1, n_tp, greet_tp, 0)
 
+    mine = pl.ds(pl.multiple_of(tp * ft, ft), ft)
     loads = [
-        (cond, CD),
-        (ctx_cond, XD),
         (shift_w, MW.at[0]),
         (scale_w, MW.at[1]),
         (gate_w, MW.at[2]),
+        (cond, CD),
+        (ctx_cond, XD),
+        (ctx_tokens.at[:, mine], CX.at[sp, :, mine]),
         (bias, BI),
         (gain, GN),
-        (ctx_tokens, CT),
         (latent, X),
         (query_w, W.at[:, pl.ds(0, att)]),
         (key_w, W.at[:, pl.ds(att, att)]),
@@ -167,120 +173,214 @@
     P1[...] = packed
     R1[sp] = packed
 
-    pl.semaphore_wait(barrier, n_sp - 1 + n_tp - 1)
-
-    def p1_copy(k):
-        peer = lax.rem(sp + k, n_sp)
+    def prepare():
+        loads[6].wait()
+        lane = lax.broadcasted_iota(jnp.int32, (COL_BLOCK, LANES), 1)
+        in_group = lax.rem(lane, STRIP)
+        query = lax.broadcasted_iota(jnp.int32, (COL_BLOCK, LANES), 0)
+        lower = (
+            jnp.maximum(query - WIN_COLS // 2, 0),
+            query,
+            jnp.minimum(query + WIN_COLS // 2, WIN_COLS),
+        )
+        inside = [(in_group >= lo) & (in_group < lo + WIN_COLS) for lo in lower]
+        offsets = 2 * WIN_ROWS - 1
+        PAD[...] = jnp.zeros_like(PAD)
+        for h in range(2):
+            PAD[h, pl.ds(0, offsets), pl.ds(0, 2 * WIN_COLS - 1)] = BI[:, h]
+            x = PAD[h]
+            x = x + pltpu.roll(x, 32, 1)
+            PAD[h] = x + pltpu.roll(x, 64, 1)
+
+        def lay_out(o, c):
+            for h in range(2):
+                line = jnp.broadcast_to(PAD[h, pl.ds(o, 1), :], (COL_BLOCK, LANES))
+                for v in range(3):
+                    turned = pltpu.roll(line, (-SHIFTS[v]) % LANES, 1, stride=1, stride_axis=0)
+                    TP[v, h, o] = jnp.where(inside[v], turned, MASKED)
+            return c
+
+        lax.fori_loop(0, offsets, lay_out, 0)
+        group = lane // STRIP
+        per = LANES // STRIP
+        variants = (
+            (-HALO, lambda i: i),
+            (0, lambda i: 0),
+            (-crows, lambda i: max(crows + i - HALO, 0)),
+            (-(urows - crows), lambda i: urows - WIN_ROWS),
+        )
+
+        def assemble(vh, c):
+            v, h = vh // 2, lax.rem(vh, 2)
+            for rv, (delta, first) in enumerate(variants):
+                for i in range(crows):
+                    for g in range(TB.shape[-1] // LANES):
+                        tile = jnp.full((COL_BLOCK, LANES), MASKED, f32)
+                        for l in range(per):
+                            j = g * per + l
+                            if first(i) <= j < first(i) + WIN_ROWS and j < urows:
+                                o = delta + j - i + WIN_ROWS - 1
+                                tile = jnp.where(group == l, TP[v, h, o], tile)
+                        TB[rv, v, i, h, :, pl.ds(g * LANES, LANES)] = tile
+            return c
+
+        lax.fori_loop(0, 6, assemble, 0)
+
+        loads[8].wait()
+
+        def norms(k, c):
+            for u in range(4):
+                at = pl.ds(pl.multiple_of(k * 64 + u * 16, 16), 16)
+                x = X[at, :].astype(f32)
+                mean = jnp.sum(x * x, axis=1, keepdims=True) * (1.0 / width)
+                RS[at, :] = jnp.broadcast_to(lax.rsqrt(mean + EPS), (16, LANES))
+            return c
+
+        lax.fori_loop(0, tokens // 64, norms, 0)
+        loads[7].wait()
+        for copy in loads[9:12]:
+            copy.wait()
+
+        CV[:, pl.ds(LANES, LANES)] = jnp.ones((CV.shape[0], LANES), bf16)
+
+        def fill(r, c):
+            for b in range(BLOCKS):
+                VS[b, r, :, pl.ds(LANES, LANES)] = jnp.ones((STRIP, LANES), bf16)
+            return c
+
+        lax.fori_loop(0, rows + 2 * HALO, fill, 0)
+
+    loads[5].wait()
+    pl.semaphore_wait(barrier, sp + n_tp - 1)
+    first_half = n_sp // 2
+    partner = tp + 1 - 2 * lax.rem(tp, 2)
+
+    def p1_copy(source):
         return pltpu.make_async_remote_copy(
             src_ref=P1,
-            dst_ref=R1.at[sp],
-            send_sem=p1_send.at[peer],
-            recv_sem=p1_recv.at[sp],
+            dst_ref=R1.at[source],
+            send_sem=p1_send.at[0],
+            recv_sem=p1_recv.at[source],
+            device_id={"sp": 0},
+            device_id_type=MESH,
+        )
+
+    def t_copy(peer):
+        return pltpu.make_async_remote_copy(
+            src_ref=P2,
+            dst_ref=P2,
+            send_sem=t_send.at[peer],
+            recv_sem=t_recv.at[0],
             device_id={"sp": peer},
             device_id_type=MESH,
         )
 
-    def p1_arrival(k):
-        peer = lax.rem(sp + k, n_sp)
+    def c_copy(peer, slot):
         return pltpu.make_async_remote_copy(
-            src_ref=P1,
-            dst_ref=R1.at[peer],
-            send_sem=p1_send.at[peer],
-            recv_sem=p1_recv.at[peer],
+            src_ref=CX.at[sp, :, mine],
+            dst_ref=CX.at[slot, :, mine],
+            send_sem=c_send.at[peer],
+            recv_sem=c_recv.at[slot],
             device_id={"sp": peer},
             device_id_type=MESH,
         )
 
-    def p1_start(k, c):
-        p1_copy(k).start()
-        return c
-
-    lax.fori_loop(1, n_sp, p1_start, 0)
-
-    loads[5].wait()
-    lane = lax.broadcasted_iota(jnp.int32, (COL_BLOCK, LANES), 1)
-    in_group = lax.rem(lane, STRIP)
-    query = lax.broadcasted_iota(jnp.int32, (COL_BLOCK, LANES), 0)
-    lower = (
-        jnp.maximum(query - WIN_COLS // 2, 0),
-        query,
-        jnp.minimum(query + WIN_COLS // 2, WIN_COLS),
-    )
-    inside = [(in_group >= lo) & (in_group < lo + WIN_COLS) for lo in lower]
-    offsets = 2 * WIN_ROWS - 1
-    PAD[...] = jnp.zeros_like(PAD)
-    for h in range(2):
-        PAD[h, pl.ds(0, offsets), pl.ds(0, 2 * WIN_COLS - 1)] = BI[h]
-        x = PAD[h]
-        x = x + pltpu.roll(x, 32, 1)
-        PAD[h] = x + pltpu.roll(x, 64, 1)
-
-    def lay_out(o, c):
-        for h in range(2):
-            line = jnp.broadcast_to(PAD[h, pl.ds(o, 1), :], (COL_BLOCK, LANES))
-            for v in range(3):
-                turned = pltpu.roll(line, (-SHIFTS[v]) % LANES, 1, stride=1, stride_axis=0)
-                TP[v, h, o] = jnp.where(inside[v], turned, MASKED)
-        return c
-
-    lax.fori_loop(0, offsets, lay_out, 0)
-    group = lane // STRIP
-    per = LANES // STRIP
-    variants = (
-        (-HALO, lambda i: i),
-        (0, lambda i: 0),
-        (-crows, lambda i: max(crows + i - HALO, 0)),
-        (-(urows - crows), lambda i: urows - WIN_ROWS),
-    )
-
-    def assemble(vh, c):
-        v, h = vh // 2, lax.rem(vh, 2)
-        for rv, (delta, first) in enumerate(variants):
-            for i in range(crows):
-                for g in range(TB.shape[-1] // LANES):
-                    tile = jnp.full((COL_BLOCK, LANES), MASKED, f32)
-                    for l in range(per):
-                        j = g * per + l
-                        if first(i) <= j < first(i) + WIN_ROWS and j < urows:
-                            o = delta + j - i + WIN_ROWS - 1
-                            tile = jnp.where(group == l, TP[v, h, o], tile)
-                    TB[rv, v, i, h, :, pl.ds(g * LANES, LANES)] = tile
-        return c
-
-    lax.fori_loop(0, 6, assemble, 0)
-
-    loads[8].wait()
-
-    def norms(k, c):
-        at = pl.ds(pl.multiple_of(k * 16, 16), 16)
-        x = X[at, :].astype(f32)
-        mean = jnp.sum(x * x, axis=1, keepdims=True) * (1.0 / width)
-        RS[at, :] = jnp.broadcast_to(lax.rsqrt(mean + EPS), (16, LANES))
-        return c
-
-    lax.fori_loop(0, tokens // 16, norms, 0)
-    loads[6].wait()
-    loads[7].wait()
-    for copy in loads[9:12]:
-        copy.wait()
-
-    CV[:, pl.ds(LANES, LANES)] = jnp.ones((CV.shape[0], LANES), bf16)
-
-    def fill(r, c):
-        for b in range(BLOCKS):
-            VS[b, r, :, pl.ds(LANES, LANES)] = jnp.ones((STRIP, LANES), bf16)
-        return c
-
-    lax.fori_loop(0, rows + 2 * HALO, fill, 0)
-
-    def p1_wait(k, c):
-        p1_arrival(k).wait_recv()
-        return c
-
-    lax.fori_loop(1, n_sp, p1_wait, 0)
-    summed = jnp.sum(R1[...], axis=0)
-    P2[...] = summed
-    R2[tp] = summed
+    def columns(piece, slot):
+        span = pl.ds(piece * first_half, first_half)
+        return CX.at[span, :, pl.ds(pl.multiple_of(slot * ft, ft), ft)]
+
+    def x_copy(piece, peer, slot):
+        return pltpu.make_async_remote_copy(
+            src_ref=columns(piece, slot),
+            dst_ref=columns(piece, slot),
+            send_sem=x_send.at[piece * n_tp + peer],
+            recv_sem=x_recv.at[piece * n_tp + slot],
+            device_id={"tp": peer},
+            device_id_type=MESH,
+        )
+
+    def d_copy(piece, slot, at):
+        return pltpu.make_async_remote_copy(
+            src_ref=columns(piece, slot),
+            dst_ref=columns(piece, slot),
+            send_sem=d_send.at[piece * n_tp + at],
+            recv_sem=d_recv.at[piece * n_tp + at],
+            device_id={"tp": partner},
+            device_id_type=MESH,
+        )
+
+    chips = n_tp // 2
+
+    def far(k):
+        return lax.rem(tp + 2 * k, n_tp)
+
+    @pl.when(sp > 0)
+    def _():
+        p1_copy(sp).start()
+
+    def tell(k, c):
+        pl.semaphore_signal(ready.at[sp], inc=1, device_id={"sp": k}, device_id_type=MESH)
+        return c
+
+    def send_back(k, c):
+        c_copy(k, sp).start()
+        return c
+
+    lax.fori_loop(0, sp, tell, 0)
+    lax.fori_loop(0, sp, send_back, 0)
+
+    prepare()
+
+    def send_on(j, c):
+        pl.semaphore_wait(ready.at[j], 1)
+        c_copy(j, sp).start()
+        return c
+
+    def send_late(j, c):
+        @pl.when(sp > 0)
+        def _():
+            pl.semaphore_wait(ready.at[j], 1)
+
+        c_copy(j, sp).start()
+        return c
+
+    def arrive(j, c):
+        @pl.when(j != sp)
+        def _():
+            c_copy(j, j).wait_recv()
+
+        return c
+
+    def pass_on(piece):
+        lax.fori_loop(piece * first_half, (piece + 1) * first_half, arrive, 0)
+        for k in range(1, chips):
+            x_copy(piece, far(k), tp).start()
+        d_copy(piece, tp, 0).start()
+
+    def hand_over(piece):
+        for k in range(1, chips):
+            x_copy(piece, far(k), far(k)).wait_recv()
+            d_copy(piece, far(k), k).start()
+
+    @pl.when(sp < first_half)
+    def _():
+        lax.fori_loop(sp + 1, first_half, send_on, 0)
+        pass_on(0)
+
+    @pl.when(sp == 0)
+    def _():
+        def p1_wait(j, c):
+            p1_copy(j).wait_recv()
+            return c
+
+        lax.fori_loop(1, n_sp, p1_wait, 0)
+        P2[...] = jnp.sum(R1[...], axis=0)
+
+    @pl.when(sp > 0)
+    def _():
+        t_copy(0).wait_recv()
+
+    R2[tp] = P2[...]
 
     def p2_copy(k, slot):
         peer = lax.rem(tp + k, n_tp)
@@ -299,62 +399,67 @@
 
     lax.fori_loop(1, n_tp, p2_start, 0)
 
+    @pl.when(sp == 0)
+    def _():
+        def early(j, c):
+            t_copy(j).start()
+            return c
+
+        def late(j, c):
+            pl.semaphore_wait(ready.at[j], 1)
+            t_copy(j).start()
+            return c
+
+        lax.fori_loop(1, first_half, early, 0)
+        lax.fori_loop(first_half, n_sp, late, 0)
+
+    lax.fori_loop(jnp.maximum(sp + 1, first_half), n_sp, send_late, 0)
+
+    @pl.when(sp >= first_half)
+    def _():
+        pass_on(0)
+
+    pass_on(1)
+    hand_over(0)
+
     def p2_wait(k, c):
         p2_copy(k, 1).wait_recv()
         return c
 
     lax.fori_loop(1, n_tp, p2_wait, 0)
 
-    ctx_rows = CT.shape[0]
-    sq = jnp.zeros((ctx_rows, 1), f32)
-    for t in range(n_tp):
-        x = CT[:, pl.ds(t * ft, ft)].astype(f32)
-        sq = sq + jnp.sum(x * x, axis=1, keepdims=True)
-    ctx_scale = lax.rsqrt(sq * (1.0 / width) + EPS)
-    r16 = lax.broadcasted_iota(jnp.int32, (16, ft), 0)
+    r32 = lax.broadcasted_iota(jnp.int32, (32, ft), 0)
     for t in range(n_tp):
         cols = pl.ds(t * ft, ft)
-        x = CT[:, cols].astype(f32) * ctx_scale
-        x = x * GN[pl.ds(t, 1), :].astype(f32) * (1.0 + R2[t, 4:5, :]) + R2[t, 3:4, :]
-        LH[pl.ds(0, ctx_rows), cols] = x.astype(bf16)
-        shift = R2[t, 0:1, :]
-        high = shift.astype(bf16).astype(f32)
-        low = shift - high
-        pair = jnp.where(r16 == 0, high, jnp.where(r16 == 1, low, 0.0))
-        LH[pl.ds(ctx_rows, 16), cols] = pair.astype(bf16)
+        quad = jnp.zeros((32, ft), f32)
+        for r, row in ((0, 0), (2, 3)):
+            shift = R2[t, row : row + 1, :]
+            high = shift.astype(bf16).astype(f32)
+            quad = jnp.where(r32 == r, high, jnp.where(r32 == r + 1, shift - high, quad))
+        LH[:, cols] = quad.astype(bf16)
     side = dot(LH[...], W[...])
-    CS[...] = side[:ctx_rows, att:].astype(bf16)
-    add = side[ctx_rows : ctx_rows + 1] + side[ctx_rows + 1 : ctx_rows + 2]
-
-    def c_copy(k, slot):
-        peer = lax.rem(sp + k, n_sp)
-        return pltpu.make_async_remote_copy(
-            src_ref=CS,
-            dst_ref=CR.at[sp if slot is None else peer],
-            send_sem=c_send.at[peer],
-            recv_sem=c_recv.at[sp if slot is None else peer],
-            device_id={"sp": peer},
-            device_id_type=MESH,
-        )
-
-    def c_start(k, c):
-        c_copy(k, None).start()
-        return c
-
-    lax.fori_loop(1, n_sp, c_start, 0)
-    CR[sp] = CS[...]
+    add = side[0:1] + side[1:2]
+    ctx_add = side[2:3] + side[3:4]
 
     halves = ft // LANES
-    scale = jnp.concatenate([R2[t, 1:2, :] for t in range(n_tp)], axis=0)
-    factor = GN[...].astype(f32) * (1.0 + scale)
-    slabs = [factor[:, s * LANES : (s + 1) * LANES] for s in range(halves)]
-    slabs.append(jnp.zeros((LANES - halves * n_tp, LANES), f32))
+    per_slab = width // LANES
+
+    def factors(row):
+        rows_ = [
+            R2[t, row : row + 1, s * LANES : (s + 1) * LANES]
+            for t in range(n_tp)
+            for s in range(halves)
+        ]
+        return GN[...].astype(f32) * (1.0 + jnp.concatenate(rows_, axis=0))
+
+    slabs = [factors(1), factors(4), jnp.zeros((LANES - 2 * per_slab, LANES), f32)]
     turned = jnp.concatenate(slabs, axis=0).T
-    for s in range(halves):
-        for t in range(n_tp):
-            at = pl.ds(t * ft + s * LANES, LANES)
-            column = turned[:, s * n_tp + t : s * n_tp + t + 1]
-            W2[at, :] = (W[at, :].astype(f32) * column).astype(bf16)
+    for k in range(per_slab):
+        at = pl.ds(k * LANES, LANES)
+        W2[at, :] = (W[at, :].astype(f32) * turned[:, k : k + 1]).astype(bf16)
+        W3[at, :] = (
+            W[at, pl.ds(att, 2 * att)].astype(f32) * turned[:, per_slab + k : per_slab + k + 1]
+        ).astype(bf16)
 
     per_block = HALO * GRID_W
     steps = rows // HALO
@@ -409,15 +514,24 @@
     def _():
         h_copy(1).start()
 
-    lax.fori_loop(2, steps, project, 0)
-
-    def c_wait(k, c):
-        c_copy(k, 1).wait_recv()
-        return c
-
-    lax.fori_loop(1, n_sp, c_wait, 0)
+    lax.fori_loop(2, 4, project, 0)
+    hand_over(1)
+    lax.fori_loop(4, steps, project, 0)
+
+    for piece in range(2):
+        for k in range(chips):
+            d_copy(piece, lax.rem(partner + 2 * k, n_tp), k).wait_recv()
+    ctx_rows = CX.shape[1]
+    pairs = dot(CX[...].reshape(n_sp * ctx_rows, width), W3[...])
     for s in range(n_sp):
-        CV[pl.ds(s * ctx_rows, ctx_rows), pl.ds(0, att)] = CR[s, :, pl.ds(att, att)]
+        x = CX[s].astype(f32)
+        mean = jnp.sum(x * x, axis=1, keepdims=True) * (1.0 / width)
+        own = pl.ds(s * ctx_rows, ctx_rows)
+        pair = (
+            pairs[s * ctx_rows : (s + 1) * ctx_rows] * lax.rsqrt(mean + EPS) + ctx_add[:, att:]
+        ).astype(bf16)
+        CK[own, :] = pair[:, :att]
+        CV[own, pl.ds(0, att)] = pair[:, att:]
 
     loads[12].wait()
 
@@ -473,7 +587,7 @@
             near = dot_nt(q2, ks)
             table = TB[rv, VARIANT[b], :, :, :, pl.ds(0, ukeys)].reshape(qrows, ukeys)
             near = near + table
-            far = dot_nt(q2, CR[:, :, pl.ds(0, att)].reshape(n_sp * ctx_rows, att))
+            far = dot_nt(q2, CK[...])
             peak = jnp.maximum(
                 jnp.max(near, axis=1, keepdims=True), jnp.max(far, axis=1, keepdims=True)
             )
@@ -513,12 +627,26 @@
         store.start()
         stores.append(store)
 
-    def p1_done(k, c):
-        p1_copy(k).wait_send()
-        c_copy(k, None).wait_send()
-        return c
-
-    lax.fori_loop(1, n_sp, p1_done, 0)
+    @pl.when(sp > 0)
+    def _():
+        p1_copy(sp).wait_send()
+
+    @pl.when(sp == 0)
+    def _():
+        def t_done(j, c):
+            t_copy(j).wait_send()
+            return c
+
+        lax.fori_loop(1, n_sp, t_done, 0)
+
+    def c_done(j, c):
+        @pl.when(j != sp)
+        def _():
+            c_copy(j, sp).wait_send()
+
+        return c
+
+    lax.fori_loop(0, n_sp, c_done, 0)
 
     def p2_done(k, c):
         p2_copy(k, None).wait_send()
@@ -526,6 +654,11 @@
         return c
 
     lax.fori_loop(1, n_tp, p2_done, 0)
+    for piece in range(2):
+        d_copy(piece, tp, 0).wait_send()
+        for k in range(1, chips):
+            x_copy(piece, far(k), tp).wait_send()
+            d_copy(piece, far(k), k).wait_send()
 
     @pl.when(sp < n_sp - 1)
     def _():
@@ -573,25 +706,24 @@
         shift_weight,
         scale_weight,
         gate_weight,
-        norm_gain.reshape(n_tp, ft),
+        norm_gain.reshape(n_sp, inputs),
         query_weight,
         key_weight,
         value_weight,
         out_weight,
-        offset_bias,
+        jnp.transpose(offset_bias, (1, 0, 2)),
     )
     dma = pltpu.SemaphoreType.DMA
     scratch = [
         pltpu.VMEM((tokens, width), bf16),
         pltpu.VMEM((n_sp, inputs), bf16),
         pltpu.VMEM((n_sp, inputs), bf16),
-        pltpu.VMEM((ctx_rows, width), bf16),
         pltpu.VMEM((3, inputs, ft), bf16),
-        pltpu.VMEM((n_tp, ft), bf16),
+        pltpu.VMEM((n_sp, inputs), bf16),
         pltpu.VMEM((width, 3 * att), bf16),
         pltpu.VMEM((width, 3 * att), bf16),
         pltpu.VMEM(out_weight.shape, bf16),
-        pltpu.VMEM(offset_bias.shape, f32),
+        pltpu.VMEM((offset_bias.shape[1], 2, offset_bias.shape[2]), f32),
         pltpu.VMEM((2, 16, LANES), f32),
         pltpu.VMEM((3, 2, 2 * WIN_ROWS, COL_BLOCK, LANES), f32),
         pltpu.VMEM((4, 3, crows, 2, COL_BLOCK, table), f32),
@@ -600,9 +732,10 @@
         pltpu.VMEM((n_sp, 8, ft), f32),
         pltpu.VMEM((8, ft), f32),
         pltpu.VMEM((n_tp, 8, ft), f32),
-        pltpu.VMEM((ctx_rows + 16, width), bf16),
-        pltpu.VMEM((ctx_rows, 2 * att), bf16),
-        pltpu.VMEM((n_sp, ctx_rows, 2 * att), bf16),
+        pltpu.VMEM((32, width), bf16),
+        pltpu.VMEM((width, 2 * att), bf16),
+        pltpu.VMEM((n_sp, ctx_rows, width), bf16),
+        pltpu.VMEM((n_sp * ctx_rows, att), bf16),
         pltpu.VMEM((n_sp * ctx_rows, 2 * LANES), bf16),
         pltpu.VMEM((BLOCKS, rows, 2, COL_BLOCK, LANES), bf16),
         pltpu.VMEM((BLOCKS, padded, STRIP, LANES), bf16),
@@ -619,6 +752,13 @@
         dma((n_tp,)),
         dma((n_sp,)),
         dma((n_sp,)),
+        dma((2 * n_tp,)),
+        dma((2 * n_tp,)),
+        dma((2 * n_tp,)),
+        dma((2 * n_tp,)),
+        dma((n_sp,)),
+        dma((1,)),
+        pltpu.SemaphoreType.REGULAR((n_sp,)),
         dma((2,)),
         dma((2,)),
         dma((n_tp,)),

time: 70.4 us -> 59.9 us (0.85)
  Pallas kernels: 65.2 us -> 57.7 us
  local copies, waits for them, and re-layouts: 4.69 us -> 2.09 us
    pallas_call x1, Pallas kernels: 65.2 us -> 57.7 us  [local(): pl.pallas_call(functools.partial(kernel, n_sp, n_tp), out_shape=jax.Shape...]
    unnamed x2 -> x1, local copies, waits for them, and re-layouts: 3.41 us -> 2.09 us
    reshape x1 -> x0, local copies, waits for them, and re-layouts: 1.28 us -> none  [local(): norm_gain.reshape(n_tp, ft)]
where the time goes in v1:
time: 59.9 us; the launch traced here: 59.8 us
  Pallas kernels  57.7 us (96%)
  local copies, waits for them, and re-layouts  2.09 us (3%)
    pallas_call x1, Pallas kernels, local(): pl.pallas_call(functools.partial(kernel, n_sp, n_tp), out_shape=jax.Shape...  57.7 us
    unnamed x1, local copies, waits for them, and re-layouts  2.09 us

profile of v1, /device:TPU:33, one launch (start us, length us, event | category | flops | bytes accessed | tf_op | source)
XLA Modules:
  0.0 59.8 jit_solution(638765669287926684)
XLA Ops:
  0.0 57.7 %shard_map.127 = bf16[192,2048]{1,0:T(8,128)(2,1)} custom-call(bf16[1536,2048]{1,0:T(8,128)(2,1)} %latent.1, bf16[16,128]{1,0:T(8,128)(2,1)} %bitcast.5, bf16[16,2048]{1,0:T(8,128)(2,1)} %ctx_tokens.1, bf16[16,128]{1,0:T(8,128)(2,1)} %bitcast.6, bf16[128,256]{1,0:T(8,128)(2,1)} %shift_w.1, bf16[128,256]{1,0:T(8,128)(2,1)} %scale_w.1, ...), custom_call_target="tpu_custom_call" | custom-call | tf_op jit(solution)/shard_map/pallas_call | solution.py:768
  57.7 2.1 %copy.15 = bf16[192,2048]{1,0:T(8,128)(2,1)} copy(bf16[192,2048]{1,0:T(8,128)(2,1)} %shard_map.127) | data formatting | bytes 1572864

commit v2 on v1

--- a/solution.py
+++ b/solution.py
@@ -18,6 +18,7 @@
 STARTS = (0, 8, 24, 32)
 VARIANT = (0, 1, 1, 2)
 SHIFTS = (15, 7, -1)
+LEADERS = 1
 EPS = 1e-6
 MASKED = -1e30
 LANES = 128
@@ -81,7 +82,6 @@
     HR,
     AS,
     AR,
-    OB,
     load_sem,
     p1_send,
     p1_recv,
@@ -100,7 +100,6 @@
     h_recv,
     a_send,
     a_recv,
-    o_sem,
 ):
     sp = lax.axis_index("sp")
     tp = lax.axis_index("tp")
@@ -173,7 +172,7 @@
     P1[...] = packed
     R1[sp] = packed
 
-    def prepare():
+    def lay_tables():
         loads[6].wait()
         lane = lax.broadcasted_iota(jnp.int32, (COL_BLOCK, LANES), 1)
         in_group = lax.rem(lane, STRIP)
@@ -226,6 +225,8 @@
 
         lax.fori_loop(0, 6, assemble, 0)
 
+
+    def prepare():
         loads[8].wait()
 
         def norms(k, c):
@@ -255,13 +256,13 @@
     first_half = n_sp // 2
     partner = tp + 1 - 2 * lax.rem(tp, 2)
 
-    def p1_copy(source):
+    def p1_copy(peer, source):
         return pltpu.make_async_remote_copy(
             src_ref=P1,
             dst_ref=R1.at[source],
-            send_sem=p1_send.at[0],
+            send_sem=p1_send.at[peer],
             recv_sem=p1_recv.at[source],
-            device_id={"sp": 0},
+            device_id={"sp": peer},
             device_id_type=MESH,
         )
 
@@ -314,9 +315,11 @@
     def far(k):
         return lax.rem(tp + 2 * k, n_tp)
 
-    @pl.when(sp > 0)
-    def _():
-        p1_copy(sp).start()
+    for leader in range(LEADERS):
+
+        @pl.when(sp > leader)
+        def _(leader=leader):
+            p1_copy(leader, sp).start()
 
     def tell(k, c):
         pl.semaphore_signal(ready.at[sp], inc=1, device_id={"sp": k}, device_id_type=MESH)
@@ -327,17 +330,29 @@
         return c
 
     lax.fori_loop(0, sp, tell, 0)
+    lay_tables()
     lax.fori_loop(0, sp, send_back, 0)
-
     prepare()
+
+    middle = 5 * n_sp // 8
+    leads = sp < LEADERS
+    if LEADERS == 1:
+        middle = n_sp
+    begins = jnp.where(sp == LEADERS - 1, LEADERS, jnp.where(sp == 0, middle, n_sp))
+    ends = jnp.where(sp == LEADERS - 1, middle, n_sp)
 
     def send_on(j, c):
         pl.semaphore_wait(ready.at[j], 1)
+
+        @pl.when(leads & (j < LEADERS))
+        def _():
+            p1_copy(j, sp).start()
+
         c_copy(j, sp).start()
         return c
 
     def send_late(j, c):
-        @pl.when(sp > 0)
+        @pl.when((j < begins) | (j >= ends))
         def _():
             pl.semaphore_wait(ready.at[j], 1)
 
@@ -365,18 +380,24 @@
     @pl.when(sp < first_half)
     def _():
         lax.fori_loop(sp + 1, first_half, send_on, 0)
+
+    @pl.when((sp < first_half) & jnp.logical_not(leads))
+    def _():
         pass_on(0)
 
-    @pl.when(sp == 0)
+    @pl.when(leads)
     def _():
         def p1_wait(j, c):
-            p1_copy(j).wait_recv()
+            @pl.when(j != sp)
+            def _():
+                p1_copy(j, j).wait_recv()
+
             return c
 
-        lax.fori_loop(1, n_sp, p1_wait, 0)
+        lax.fori_loop(0, n_sp, p1_wait, 0)
         P2[...] = jnp.sum(R1[...], axis=0)
 
-    @pl.when(sp > 0)
+    @pl.when(jnp.logical_not(leads))
     def _():
         t_copy(0).wait_recv()
 
@@ -399,28 +420,22 @@
 
     lax.fori_loop(1, n_tp, p2_start, 0)
 
-    @pl.when(sp == 0)
-    def _():
-        def early(j, c):
-            t_copy(j).start()
-            return c
-
-        def late(j, c):
+    def share_sums(j, c):
+        @pl.when(j >= first_half)
+        def _():
             pl.semaphore_wait(ready.at[j], 1)
-            t_copy(j).start()
-            return c
-
-        lax.fori_loop(1, first_half, early, 0)
-        lax.fori_loop(first_half, n_sp, late, 0)
-
+
+        t_copy(j).start()
+        return c
+
+    lax.fori_loop(begins, ends, share_sums, 0)
     lax.fori_loop(jnp.maximum(sp + 1, first_half), n_sp, send_late, 0)
 
-    @pl.when(sp >= first_half)
+    @pl.when((sp >= first_half) | leads)
     def _():
         pass_on(0)
 
     pass_on(1)
-    hand_over(0)
 
     def p2_wait(k, c):
         p2_copy(k, 1).wait_recv()
@@ -460,6 +475,8 @@
         W3[at, :] = (
             W[at, pl.ds(att, 2 * att)].astype(f32) * turned[:, per_slab + k : per_slab + k + 1]
         ).astype(bf16)
+
+    hand_over(0)
 
     per_block = HALO * GRID_W
     steps = rows // HALO
@@ -581,20 +598,23 @@
         base = jnp.where(
             (rv == 1) | (rv == 2), HALO, jnp.where(rv == 3, rows + HALO - urows, c * crows)
         )
+        qs = [QS[b, pl.ds(c * crows, crows)].reshape(qrows, LANES) for b in range(BLOCKS)]
+        fars = dot_nt(jnp.concatenate(qs, axis=0), CK[...])
+        near_exps, far_exps = [], []
         for b in range(BLOCKS):
-            q2 = QS[b, pl.ds(c * crows, crows)].reshape(qrows, LANES)
             ks = KS[b, pl.ds(base, urows)].reshape(ukeys, LANES)
-            near = dot_nt(q2, ks)
             table = TB[rv, VARIANT[b], :, :, :, pl.ds(0, ukeys)].reshape(qrows, ukeys)
-            near = near + table
-            far = dot_nt(q2, CK[...])
+            near = dot_nt(qs[b], ks) + table
+            far = fars[b * qrows : (b + 1) * qrows]
             peak = jnp.maximum(
                 jnp.max(near, axis=1, keepdims=True), jnp.max(far, axis=1, keepdims=True)
             )
-            near = jnp.exp(near - peak).astype(bf16)
-            far = jnp.exp(far - peak).astype(bf16)
+            near_exps.append(jnp.exp(near - peak).astype(bf16))
+            far_exps.append(jnp.exp(far - peak).astype(bf16))
+        far_sums = dot(jnp.concatenate(far_exps, axis=0), CV[...])
+        for b in range(BLOCKS):
             vs = VS[b, pl.ds(base, urows)].reshape(ukeys, 2 * LANES)
-            both = dot(near, vs) + dot(far, CV[...])
+            both = dot(near_exps[b], vs) + far_sums[b * qrows : (b + 1) * qrows]
             value = (both[:, :LANES] / both[:, LANES:]).reshape(crows, 2, COL_BLOCK, LANES)
             for i in range(crows):
                 AS[c, pl.ds(i * GRID_W + b * COL_BLOCK, COL_BLOCK), :] = jnp.where(
@@ -618,26 +638,25 @@
     lax.fori_loop(1, n_tp, a_wait, 0)
     merged = jnp.concatenate([AR[t] for t in range(n_tp)], axis=1)
     own = pl.ds(pl.multiple_of(tp * share, share), share)
-    stores = []
     for t in range(n_tp):
         cols = pl.ds(t * ft, ft)
         branch = dot(merged, WO[:, cols])
-        OB[:, cols] = (X[own, cols].astype(f32) + R2[t, 2:3, :] * branch).astype(bf16)
-        store = pltpu.make_async_copy(OB.at[:, cols], out.at[:, cols], o_sem.at[t])
-        store.start()
-        stores.append(store)
-
-    @pl.when(sp > 0)
-    def _():
-        p1_copy(sp).wait_send()
-
-    @pl.when(sp == 0)
-    def _():
-        def t_done(j, c):
-            t_copy(j).wait_send()
-            return c
-
-        lax.fori_loop(1, n_sp, t_done, 0)
+        out[:, cols] = (X[own, cols].astype(f32) + R2[t, 2:3, :] * branch).astype(bf16)
+
+    def p1_done(j, c):
+        @pl.when(j != sp)
+        def _():
+            p1_copy(j, sp).wait_send()
+
+        return c
+
+    lax.fori_loop(0, LEADERS, p1_done, 0)
+
+    def t_done(j, c):
+        t_copy(j).wait_send()
+        return c
+
+    lax.fori_loop(begins, ends, t_done, 0)
 
     def c_done(j, c):
         @pl.when(j != sp)
@@ -667,9 +686,6 @@
     @pl.when(sp > 0)
     def _():
         h_copy(1).wait_send()
-
-    for store in stores:
-        store.wait()
 
 
 def local(n_sp, n_tp, *args):
@@ -744,7 +760,6 @@
         pltpu.VMEM((2, HALO * GRID_W, 2 * att), bf16),
         pltpu.VMEM((n_tp, share, LANES), bf16),
         pltpu.VMEM((n_tp, share, LANES), bf16),
-        pltpu.VMEM((share, width), bf16),
         dma((13,)),
         dma((n_sp,)),
         dma((n_sp,)),
@@ -763,16 +778,16 @@
         dma((2,)),
         dma((n_tp,)),
         dma((n_tp,)),
-        dma((n_tp,)),
     ]
+    operands = tuple(pltpu.with_memory_space_constraint(x, pltpu.HBM) for x in operands)
     return pl.pallas_call(
         functools.partial(kernel, n_sp, n_tp),
         out_shape=jax.ShapeDtypeStruct((share, width), bf16),
         in_specs=[pl.BlockSpec(memory_space=pl.ANY)] * len(operands),
-        out_specs=pl.BlockSpec(memory_space=pl.ANY),
+        out_specs=pl.BlockSpec(memory_space=pltpu.VMEM),
         scratch_shapes=scratch,
         compiler_params=pltpu.CompilerParams(
-            collective_id=0, has_side_effects=True, vmem_limit_bytes=60 * 1024 * 1024
+            collective_id=0, has_side_effects=True, vmem_limit_bytes=46_000_000
         ),
     )(*operands)
 

time: 59.9 us -> 57.3 us (0.957)
  Pallas kernels: 57.7 us -> 56.3 us
  local copies, waits for them, and re-layouts: 2.09 us -> 0.88 us
    pallas_call x1, Pallas kernels: 57.7 us -> 56.3 us  [local(): pl.pallas_call(functools.partial(kernel, n_sp, n_tp), out_shape=jax.Shape...]
    unnamed x1, local copies, waits for them, and re-layouts: 2.09 us -> 0.88 us
where the time goes in v2:
time: 57.3 us; the launch traced here: 57.2 us
  Pallas kernels  56.3 us (98%)
  local copies, waits for them, and re-layouts  0.88 us (2%)
    pallas_call x1, Pallas kernels, local(): pl.pallas_call(functools.partial(kernel, n_sp, n_tp), out_shape=jax.Shape...  56.3 us

profile of v2, /device:TPU:33, one launch (start us, length us, event | category | flops | bytes accessed | tf_op | source)
XLA Modules:
  0.0 57.2 jit_solution(12132250534277706711)
XLA Ops:
  0.0 56.3 %shard_map.127 = bf16[192,2048]{1,0:T(8,128)(2,1)S(1)} custom-call(bf16[1536,2048]{1,0:T(8,128)(2,1)} %latent.1, bf16[16,128]{1,0:T(8,128)(2,1)} %bitcast.5, bf16[16,2048]{1,0:T(8,128)(2,1)} %ctx_tokens.1, bf16[16,128]{1,0:T(8,128)(2,1)} %bitcast.6, bf16[128,256]{1,0:T(8,128)(2,1)} %shift_w.1, bf16[128,256]{1,0:T(8,128)(2,1)} %scale_w.1, ...), custom_call_target="tpu_custom_call" | custom-call | tf_op jit(solution)/shard_map/pallas_call | solution.py:783
  56.4 0.9 %copy.15 = bf16[192,2048]{1,0:T(8,128)(2,1)} copy(bf16[192,2048]{1,0:T(8,128)(2,1)S(1)} %shard_map.127) | data formatting | bytes 1572864

commit v3 on v2

--- a/solution.py
+++ b/solution.py
@@ -251,6 +251,11 @@
 
         lax.fori_loop(0, rows + 2 * HALO, fill, 0)
 
+    @pl.when(sp == 0)
+    def _():
+        lay_tables()
+        prepare()
+
     loads[5].wait()
     pl.semaphore_wait(barrier, sp + n_tp - 1)
     first_half = n_sp // 2
@@ -330,9 +335,11 @@
         return c
 
     lax.fori_loop(0, sp, tell, 0)
-    lay_tables()
-    lax.fori_loop(0, sp, send_back, 0)
-    prepare()
+    @pl.when(sp > 0)
+    def _():
+        lay_tables()
+        lax.fori_loop(0, sp, send_back, 0)
+        prepare()
 
     middle = 5 * n_sp // 8
     leads = sp < LEADERS
@@ -418,8 +425,6 @@
         p2_copy(k, None).start()
         return c
 
-    lax.fori_loop(1, n_tp, p2_start, 0)
-
     def share_sums(j, c):
         @pl.when(j >= first_half)
         def _():
@@ -428,7 +433,11 @@
         t_copy(j).start()
         return c
 
-    lax.fori_loop(begins, ends, share_sums, 0)
+    nearest = jnp.minimum(begins + 2, ends)
+    lax.fori_loop(begins, nearest, share_sums, 0)
+    lax.fori_loop(1, n_tp, p2_start, 0)
+
+    lax.fori_loop(nearest, ends, share_sums, 0)
     lax.fori_loop(jnp.maximum(sp + 1, first_half), n_sp, send_late, 0)
 
     @pl.when((sp >= first_half) | leads)
@@ -472,11 +481,6 @@
     for k in range(per_slab):
         at = pl.ds(k * LANES, LANES)
         W2[at, :] = (W[at, :].astype(f32) * turned[:, k : k + 1]).astype(bf16)
-        W3[at, :] = (
-            W[at, pl.ds(att, 2 * att)].astype(f32) * turned[:, per_slab + k : per_slab + k + 1]
-        ).astype(bf16)
-
-    hand_over(0)
 
     per_block = HALO * GRID_W
     steps = rows // HALO
@@ -531,9 +535,17 @@
     def _():
         h_copy(1).start()
 
-    lax.fori_loop(2, 4, project, 0)
+    lax.fori_loop(2, steps - 2, project, 0)
+    hand_over(0)
+    lax.fori_loop(steps - 2, steps - 1, project, 0)
     hand_over(1)
-    lax.fori_loop(4, steps, project, 0)
+    lax.fori_loop(steps - 1, steps, project, 0)
+
+    for k in range(per_slab):
+        at = pl.ds(k * LANES, LANES)
+        W3[at, :] = (
+            W[at, pl.ds(att, 2 * att)].astype(f32) * turned[:, per_slab + k : per_slab + k + 1]
+        ).astype(bf16)
 
     for piece in range(2):
         for k in range(chips):

time: 57.3 us -> 57.8 us (level)
  no operation moved by 1% of the time
where the time goes in v3:
time: 57.8 us; the launch traced here: 57.7 us
  Pallas kernels  56.8 us (98%)
  local copies, waits for them, and re-layouts  0.88 us (2%)
    pallas_call x1, Pallas kernels, local(): pl.pallas_call(functools.partial(kernel, n_sp, n_tp), out_shape=jax.Shape...  56.8 us

profile of v3, /device:TPU:33, one launch (start us, length us, event | category | flops | bytes accessed | tf_op | source)
XLA Modules:
  0.0 57.7 jit_solution(17636985907558958678)
XLA Ops:
  0.0 56.8 %shard_map.127 = bf16[192,2048]{1,0:T(8,128)(2,1)S(1)} custom-call(bf16[1536,2048]{1,0:T(8,128)(2,1)} %latent.1, bf16[16,128]{1,0:T(8,128)(2,1)} %bitcast.5, bf16[16,2048]{1,0:T(8,128)(2,1)} %ctx_tokens.1, bf16[16,128]{1,0:T(8,128)(2,1)} %bitcast.6, bf16[128,256]{1,0:T(8,128)(2,1)} %shift_w.1, bf16[128,256]{1,0:T(8,128)(2,1)} %scale_w.1, ...), custom_call_target="tpu_custom_call" | custom-call | tf_op jit(solution)/shard_map/pallas_call | solution.py:795
  56.8 0.9 %copy.15 = bf16[192,2048]{1,0:T(8,128)(2,1)} copy(bf16[192,2048]{1,0:T(8,128)(2,1)S(1)} %shard_map.127) | data formatting | bytes 1572864
